TPU v7x, 32 devices: a whole 2x2x4 slice. The times are simulated.
32 devices in a mesh: sp: 8 (over z, y), tp: 4 (over x, core).
Axes of the slice: x: 2, y: 2, z: 4, core: 2. Of those that a mesh axis runs over, the one named last changes fastest.
Arguments:
- layer_source: bfloat16 [8192, 2048], P(('sp', 'tp')), may hold values from -6 to 6
- broad_probe_tensor: bfloat16 [8192, 512], P('sp', 'tp'), may hold values from -6 to 6
- broad_retention_preact: bfloat16 [8192, 512], P('sp', 'tp'), may hold values from -6 to 6
- broad_floor_margin: float32 [512], P('tp'), may hold values from 3.6621094e-05 to 0.12
- slim_probe_tensor: bfloat16 [8192, 256], P('sp', 'tp'), may hold values from -6 to 6
- slim_retention_preact: bfloat16 [8192, 256], P('sp', 'tp'), may hold values from -6 to 6
- slim_floor_margin: float32 [256], P('tp'), may hold values from 3.6621094e-05 to 0.12
- branch_content_tensor: bfloat16 [2, 8192, 512], P(None, 'sp', 'tp'), may hold values from -6 to 6
- emitted_switch_preact: bfloat16 [2, 8192, 512], P(None, 'sp', 'tp'), may hold values from -6 to 6
- extra_log_fades: float32 [2, 8192, 4], P(None, 'sp', 'tp'), may hold values from -1.4 to 0
- channel_norm_scale: float32 [128], replicated, may hold values from 0.1 to 1.9
- emission_projection: bfloat16 [2, 512, 2048], replicated, may hold values from -0.1875 to 0.1875
- mlp_norm_scale: float32 [2048], replicated, may hold values from 0.1 to 1.9
- switch_projection: bfloat16 [2048, 5632], P('sp', 'tp'), may hold values from -0.125 to 0.125
- expand_projection: bfloat16 [2048, 5632], P('sp', 'tp'), may hold values from -0.125 to 0.125
- shrink_projection: bfloat16 [5632, 2048], P('tp', 'sp'), may hold values from -0.078125 to 0.078125
Outputs:
- layer_out: bfloat16 [8192, 2048], P(('sp', 'tp'))
All inputs are finite; a program needn't handle non-finite values.
Results may differ from a plain program's by a relative error of at most 0.0095.
Values may be sent and summed in bfloat16 or wider, within the bound.
A program may use at most 192 MiB of HBM per device.

v0:
```python
import jax
import jax.numpy as jnp
from jax import lax
from jax.sharding import PartitionSpec as P

BRANCH_CHANNELS = 4
BLOCK = 64


EPSILON = 1e-06
EXACT_PRECISION = lax.Precision.HIGHEST


def entering(part, axis, combine, identity):
    place = lax.axis_index(axis)
    gathered = jax.tree.map(lambda a: lax.all_gather(a, axis), part)
    state = jax.tree.map(lambda a, e: jnp.zeros_like(a) + jnp.asarray(e, a.dtype), part, identity)

    def one(lap, state):
        return combine(
            state, jax.tree.map(lambda a: lax.dynamic_index_in_dim(a, lap, 0, False), gathered)
        )

    return lax.fori_loop(0, place, one, state)


def switched_token_entries(
    probe_array, retention_sigmoid, floor_margin, spike_rows, rows_of_values, count_heads
):
    length = probe_array.shape[0]
    key_width = probe_array.shape[1] // count_heads
    shaped = retention_sigmoid.astype(jnp.float32).reshape(length, count_heads, key_width)
    address_entries = floor_margin.reshape(count_heads, key_width) * jax.nn.sigmoid(-shaped)
    log_fade_amount = jnp.log1p(-address_entries) + spike_rows[:, :, None]
    probe_entries = jax.nn.silu(probe_array.astype(jnp.float32)).reshape(
        length, count_heads, key_width
    ) * key_width ** (-0.5)
    content_arrays = rows_of_values.astype(jnp.float32).reshape(length, count_heads, -1)
    return (probe_entries, address_entries, log_fade_amount, content_arrays)


def block_recurrence(probe_entries, address_entries, log_fade_amount, content_arrays, block_len):
    length, count_heads, key_width = probe_entries.shape
    value_width = content_arrays.shape[2]
    block_count = length // block_len

    def to_blocks(tensor):
        return jnp.moveaxis(
            tensor.reshape(block_count, block_len, count_heads, tensor.shape[2]), 2, 1
        )

    causal_mask = jnp.tril(jnp.ones((block_len, block_len), dtype=bool))[None, :, :, None]

    def advance(carried, inputs):
        state_stack, running = carried
        block_queries, key_block, block_values, decay_block = inputs
        prefix_decay = jnp.cumsum(decay_block, axis=1)
        state_contribution = jnp.einsum(
            "yga,yau->ygu",
            block_queries * jnp.exp(prefix_decay),
            state_stack,
            precision=EXACT_PRECISION,
        )
        relative = prefix_decay[:, :, None, :] - prefix_decay[:, None, :, :]
        decays = jnp.exp(jnp.where(causal_mask, relative, -jnp.inf))
        scores = jnp.einsum(
            "htk,hsk,htsk->hts", block_queries, key_block, decays, precision=EXACT_PRECISION
        )
        inside = jnp.einsum("hts,hsv->htv", scores, block_values, precision=EXACT_PRECISION)
        total_blocks = prefix_decay[:, -1, :]
        weighted_scores = key_block * jnp.exp(total_blocks[:, None, :] - prefix_decay)
        state_stack = jnp.exp(total_blocks)[:, :, None] * state_stack + jnp.einsum(
            "xpf,xpq->xfq", weighted_scores, block_values, precision=EXACT_PRECISION
        )
        reached_state = block_queries * jnp.exp(running[:, None, :] + prefix_decay)
        return ((state_stack, running + total_blocks), (state_contribution + inside, reached_state))

    initial = (
        jnp.zeros((count_heads, key_width, value_width), jnp.float32),
        jnp.zeros((count_heads, key_width), jnp.float32),
    )
    last_carry, (output_rows, reached_state) = lax.scan(
        advance,
        initial,
        (
            to_blocks(probe_entries),
            to_blocks(address_entries),
            to_blocks(content_arrays),
            to_blocks(log_fade_amount),
        ),
    )

    def from_blocks(tensor):
        return jnp.moveaxis(tensor, 1, 2).reshape(length, count_heads, tensor.shape[3])

    return (from_blocks(output_rows), from_blocks(reached_state), last_carry)


def head_norm(output_rows, channel_norm_scale, gate_rows):
    inverse = lax.rsqrt(jnp.mean(output_rows * output_rows, axis=2, keepdims=True) + EPSILON)
    normed = (output_rows * inverse * channel_norm_scale).reshape(output_rows.shape[0], -1)
    return (normed * jax.nn.silu(gate_rows.astype(jnp.float32))).astype(jnp.bfloat16)


def combine(earlier, later):
    wide_early, wide_state_early, narrow_early, narrow_state_early = earlier
    wide_late, wide_state_late, narrow_late, narrow_state_late = later
    return (
        wide_early + wide_late,
        jnp.exp(wide_late)[:, :, None] * wide_state_early + wide_state_late,
        narrow_early + narrow_late,
        jnp.exp(narrow_late)[:, :, None] * narrow_state_early + narrow_state_late,
    )


def local(
    layer_source,
    broad_probe_tensor,
    broad_retention_preact,
    broad_floor_margin,
    slim_probe_tensor,
    slim_retention_preact,
    slim_floor_margin,
    branch_content_tensor,
    emitted_switch_preact,
    extra_log_fades,
    channel_norm_scale,
    emission_projection,
    mlp_norm_scale,
    switch_projection,
    expand_projection,
    shrink_projection,
):
    tp_count = lax.axis_size("tp")
    count_heads = BRANCH_CHANNELS // tp_count
    row_count = layer_source.shape[0]
    groups = (
        (broad_probe_tensor, broad_retention_preact, broad_floor_margin),
        (slim_probe_tensor, slim_retention_preact, slim_floor_margin),
    )
    locals_out = []
    summaries = []
    for element_ordinal in range(2):
        probe_array, retention_sigmoid, floor_margin = groups[element_ordinal]
        probe_entries, address_entries, log_fade_amount, content_arrays = switched_token_entries(
            probe_array,
            retention_sigmoid,
            floor_margin,
            extra_log_fades[element_ordinal],
            branch_content_tensor[element_ordinal],
            count_heads,
        )
        output_rows, reached_state, last_carry = block_recurrence(
            probe_entries, address_entries, log_fade_amount, content_arrays, BLOCK
        )
        locals_out.append((output_rows, reached_state))
        summaries.append(last_carry)
    wide_state, wide_log = summaries[0]
    narrow_state, narrow_log = summaries[1]
    identity = (
        jnp.zeros_like(wide_log),
        jnp.zeros_like(wide_state),
        jnp.zeros_like(narrow_log),
        jnp.zeros_like(narrow_state),
    )
    carried = entering((wide_log, wide_state, narrow_log, narrow_state), "sp", combine, identity)
    incoming_state = (carried[1], carried[3])
    mixed_parts = []
    for element_ordinal in range(2):
        output_rows, reached_state = locals_out[element_ordinal]
        output_rows = output_rows + jnp.einsum(
            "qgj,gjw->qgw",
            reached_state,
            incoming_state[element_ordinal],
            precision=EXACT_PRECISION,
        )
        mixed_parts.append(
            head_norm(output_rows, channel_norm_scale, emitted_switch_preact[element_ordinal])
        )
    mixed = jnp.concatenate(mixed_parts, axis=1)
    group_width = branch_content_tensor.shape[2]
    model_width = emission_projection.shape[2]
    regrouped = lax.all_to_all(mixed, "tp", split_axis=0, concat_axis=1, tiled=True)
    shaped = regrouped.reshape(row_count, tp_count, 2, group_width)
    branch = jnp.einsum(
        "rtgc,gtcd->rd",
        shaped,
        emission_projection.reshape(2, tp_count, group_width, model_width),
        preferred_element_type=jnp.float32,
    )
    updated = layer_source.astype(jnp.float32) + branch
    inverse = lax.rsqrt(jnp.mean(updated * updated, axis=1, keepdims=True) + EPSILON)
    normed = (updated * inverse * mlp_norm_scale).astype(jnp.bfloat16)
    gate_full, up_full, down_full = (
        lax.all_gather(switch_projection, "sp", axis=0, tiled=True),
        lax.all_gather(expand_projection, "sp", axis=0, tiled=True),
        lax.all_gather(shrink_projection, "sp", axis=1, tiled=True),
    )
    row_piece = lax.all_gather(normed, "tp", axis=0, tiled=True)
    gate_part = jnp.dot(row_piece, gate_full, preferred_element_type=jnp.float32)
    up_part = jnp.dot(row_piece, up_full, preferred_element_type=jnp.float32)
    hidden = (jax.nn.silu(gate_part) * up_part).astype(jnp.bfloat16)
    ffn_sum = lax.psum_scatter(
        jnp.dot(hidden, down_full, preferred_element_type=jnp.float32).astype(jnp.bfloat16),
        "tp",
        scatter_dimension=0,
        tiled=True,
    ).astype(jnp.float32)
    return (updated + 0.5 * ffn_sum).astype(jnp.bfloat16)


def solution(mesh):
    placed = (
        P(("sp", "tp"), None),
        P("sp", "tp"),
        P("sp", "tp"),
        P("tp"),
        P("sp", "tp"),
        P("sp", "tp"),
        P("tp"),
        P(None, "sp", "tp"),
        P(None, "sp", "tp"),
        P(None, "sp", "tp"),
        P(),
        P(),
        P(),
        P("sp", "tp"),
        P("sp", "tp"),
        P("tp", "sp"),
    )
    return jax.shard_map(
        local, mesh=mesh, in_specs=placed, out_specs=P(("sp", "tp"), None), check_vma=False
    )
```

profile of v0, /device:TPU:0, one launch (start us, length us, event | category | flops | bytes accessed | tf_op | source)
XLA Modules:
  0.0 770.1 jit_solution(4900579919354530398)
XLA Ops:
  9.6 1.8 fusion.99
  13.4 179.5 %while.51 = (s32[]{:T(128)}, f32[1,64,128]{2,1,0:T(8,128)S(1)}, f32[1,64]{1,0:T(1,128)S(1)}, f32[16,1,64,128]{3,2,1,0:T(8,128)S(1)}, f32[16,1,64,64]{3,2,1,0:T(8...) while((s32[]{:T(128)}, f32[1,64,128]{2,1,0:T(8,128)S(1)}, ...), condition=%wide.region_5.6_spmd.clone, body=%wide.region_3.5_spmd.clone.sunk | while | flops 20504708 | bytes 4946317 | solution.py:82
  15.8 1.7 select_exponential_fusion.5
  17.5 3.3 copy.114
  27.0 1.7 select_exponential_fusion.5
  28.7 3.3 copy.114
  38.2 1.7 select_exponential_fusion.5
  39.9 3.3 copy.114
  49.4 1.7 select_exponential_fusion.5
  51.1 3.3 copy.114
  60.6 1.7 select_exponential_fusion.5
  62.4 3.3 copy.114
  71.9 1.7 select_exponential_fusion.5
  73.6 3.3 copy.114
  83.1 1.7 select_exponential_fusion.5
  84.8 3.3 copy.114
  94.3 1.7 select_exponential_fusion.5
  96.0 3.3 copy.114
  105.5 1.7 select_exponential_fusion.5
  107.2 3.3 copy.114
  116.7 1.7 select_exponential_fusion.5
  118.5 3.3 copy.114
  128.0 1.7 select_exponential_fusion.5
  129.7 3.3 copy.114
  139.2 1.7 select_exponential_fusion.5
  140.9 3.3 copy.114
  150.4 1.7 select_exponential_fusion.5
  152.1 3.3 copy.114
  161.6 1.7 select_exponential_fusion.5
  163.4 3.3 copy.114
  172.9 1.7 select_exponential_fusion.5
  174.6 3.3 copy.114
  184.1 1.7 select_exponential_fusion.5
  185.8 3.3 copy.114
  192.9 32.6 %all-gather.3 = f32[8,64,128]{2,1,0:T(8,128)S(1)} all-gather(f32[1,64,128]{2,1,0:T(8,128)S(1)} %get-tuple-element.189), channel_id=5, replica_groups=mesh['sp'=8,'tp'=4] {'sp'}, dimensions={0}, use_global_device_ids=true | all-gather | bytes 294912 | tf_op jit(solution)/shard_map/all_gather | solution.py:16
  225.5 20.6 %all-gather.5 = f32[8,1,64]{2,1,0:T(1,128)S(1)} all-gather(f32[1,1,64]{2,1,0:T(1,128)S(1)} %bitcast.343), channel_id=4, replica_groups=mesh['sp'=8,'tp'=4] {'sp'}, dimensions={0}, use_global_device_ids=true | all-gather | bytes 2304 | tf_op jit(solution)/shard_map/all_gather | solution.py:16
  248.1 2.1 divide_multiply_fusion
  250.3 64.7 %while.50 = (s32[]{:T(128)}, f32[1,128,128]{2,1,0:T(8,128)S(1)}, f32[1,128]{1,0:T(1,128)S(1)}, f32[16,1,64,128]{3,2,1,0:T(8,128)S(1)}, f32[16,1,64,128]{3,2,1,0:...) while((s32[]{:T(128)}, f32[1,128,128]{2,1,0:T(8,128)S(1)}, ...), condition=%wide.region_2.3_spmd.clone, body=%wide.region_0.2_spmd.clone.sunk | while | flops 34709760 | bytes 5176981 | solution.py:82
  251.9 1.7 fusion.165
  255.9 1.7 fusion.165
  260.0 1.7 fusion.165
  264.0 1.7 fusion.165
  268.1 1.7 fusion.165
  272.1 1.7 fusion.165
  276.1 1.7 fusion.165
  280.2 1.7 fusion.165
  284.2 1.7 fusion.165
  288.3 1.7 fusion.165
  292.3 1.7 fusion.165
  296.4 1.7 fusion.165
  300.4 1.7 fusion.165
  315.1 31.3 %all-gather.1 = f32[8,128,128]{2,1,0:T(8,128)S(1)} all-gather(f32[1,128,128]{2,1,0:T(8,128)S(1)} %get-tuple-element.187), channel_id=3, replica_groups=mesh['sp'=8,'tp'=4] {'sp'}, dimensions={0}, use_global_device_ids=true | all-gather | bytes 589824 | tf_op jit(solution)/shard_map/all_gather | solution.py:16
  346.3 16.3 %all-gather.4 = f32[8,1,128]{2,1,0:T(1,128)S(1)} all-gather(f32[1,1,128]{2,1,0:T(1,128)S(1)} %bitcast.342), channel_id=2, replica_groups=mesh['sp'=8,'tp'=4] {'sp'}, dimensions={0}, use_global_device_ids=true | all-gather | bytes 4608 | tf_op jit(solution)/shard_map/all_gather | solution.py:16
  363.1 1.8 multiply_reduce_fusion.1
  366.6 11.4 %all_to_all.13 = bf16[4,256,256]{2,1,0:T(8,128)(2,1)S(1)} all-to-all(bf16[4,256,256]{2,1,0:T(8,128)(2,1)S(1)} %pad_maximum_fusion), channel_id=1, replica_groups=mesh['sp'=8,'tp'=4] {'tp'}, dimensions={0} | all-to-all | bytes 1048576 | tf_op jit(solution)/shard_map/all_to_all | solution.py:183
  378.2 3.9 multiply_reduce_fusion
  385.6 31.5 %all-gather.11.cloned.1.call-done = bf16[1024,2048]{1,0:T(8,128)(2,1)} async-done(((bf16[256,2048]{1,0:T(8,128)(2,1)}), bf16[1024,2048]{1,0:T(8,128)(2,1)}) %all-gather.11.cloned.1.call-update) | async-done | bytes 4194320 | tf_op jit(solution)/shard_map/all_gather | solution.py:199
  417.1 94.5 %all-gather.13.cloned.1.call-done = bf16[2048,1408]{1,0:T(8,128)(2,1)} async-done(((bf16[256,1408]{1,0:T(8,128)(2,1)}), bf16[2048,1408]{1,0:T(8,128)(2,1)}) %all-gather.13.cloned.1.call-update) | async-done | bytes 5767184 | tf_op jit(solution)/shard_map/all_gather | solution.py:195
  511.6 11.6 %fusion.101 = f32[1024,1408]{1,0:T(8,128)} fusion(bf16[1024,2048]{1,0:T(8,128)(2,1)} %all-gather.11.cloned.1.call-done, bf16[2048,1408]{1,0:T(8,128)(2,1)} %all-gather.13.cloned.1.call-done), kind=kOutput, calls=%fused_computation.155 | convolution fusion | flops 5905580032 | bytes 15728640 | tf_op jit(solution)/shard_map/dot_general | solution.py:200
  523.3 81.1 %all-gather.15.cloned.1.call-done = bf16[2048,1408]{1,0:T(8,128)(2,1)} async-done(((bf16[256,1408]{1,0:T(8,128)(2,1)}), bf16[2048,1408]{1,0:T(8,128)(2,1)}) %all-gather.15.cloned.1.call-update) | async-done | bytes 5767184 | tf_op jit(solution)/shard_map/all_gather | solution.py:196
  604.3 93.2 %all-gather.17.cloned.1.call-done = bf16[1408,2048]{1,0:T(8,128)(2,1)} async-done(((bf16[1408,256]{1,0:T(8,128)(2,1)}), bf16[1408,2048]{1,0:T(8,128)(2,1)}) %all-gather.17.cloned.1.call-update) | async-done | bytes 5767184 | tf_op jit(solution)/shard_map/all_gather | solution.py:197
  697.6 20.6 %convolution_convert_fusion = bf16[1024,2048]{1,0:T(8,128)(2,1)} fusion(bf16[1408,2048]{1,0:T(8,128)(2,1)} %all-gather.17.cloned.1.call-done, f32[1024,1408]{1,0:T(8,128)} %fusion.101, bf16[1024,2048]{1,0:T(8,128)(2,1)} %all-gather.11.cloned.1.call-done, bf16[2048,1408]{1,0:T(8,128)(2,1)} %all-gather.15.cloned.1.call-done), kind=kOutput, calls=%fused_computation.101 | convolution fusion | flops 11821907968 | bytes 25690112 | tf_op jit(solution)/shard_map/dot_general | solution.py:204
  718.2 42.9 %reduce-scatter.2.cloned.1.call-done = bf16[256,2048]{1,0:T(8,128)(2,1)} async-done(((bf16[1024,2048]{1,0:T(8,128)(2,1)}), bf16[256,2048]{1,0:T(8,128)(2,1)}) %reduce-scatter.2.cloned.1.call-update) | async-done | bytes 1048592 | tf_op jit(solution)/shard_map/reduce_scatter | solution.py:203
  761.1 2.5 add_convert_fusion
  (471 shorter events, 151.6 us)
Async XLA Ops:
  6.5 5.7 copy-start.1
  6.5 410.6 %all-gather.11.cloned.1.call-start = ((), (), s32[]{:S(2)}) async-start(), calls=%async_computation.2 | async-start | bytes 5242880 | tf_op jit(solution)/shard_map/all_gather | solution.py:199
  362.7 2.9 copy-start.3
  363.1 2.9 copy-start
  378.2 3.9 copy-start.2
  383.3 128.3 %all-gather.13.cloned.1.call-start = ((), (), s32[]{:S(2)}) async-start(), calls=%async_computation.3 | async-start | bytes 6488064 | tf_op jit(solution)/shard_map/all_gather | solution.py:195
  384.1 220.3 %all-gather.15.cloned.1.call-start = ((), (), s32[]{:S(2)}) async-start(), calls=%async_computation.4 | async-start | bytes 6488064 | tf_op jit(solution)/shard_map/all_gather | solution.py:196
  384.8 312.8 %all-gather.17.cloned.1.call-start = ((), (), s32[]{:S(2)}) async-start(), calls=%async_computation.5 | async-start | bytes 6488064 | tf_op jit(solution)/shard_map/all_gather | solution.py:197
  385.4 375.7 %reduce-scatter.2.cloned.1.call-start = ((), (), s32[]{:S(2)}) async-start(), calls=%async_computation.6 | async-start | bytes 5242880 | tf_op jit(solution)/shard_map/reduce_scatter | solution.py:203
Sparse Core Ops, SparseCore 0:
  383.4 33.6 all-gather.10
  419.3 92.3 all-gather.12
  513.8 90.4 all-gather.14
  606.2 91.2 all-gather.16
  718.3 42.7 reduce-scatter.1
where the time goes:
time: 777 us; the launch traced here: 770 us
  waiting for transfers between devices  345 us (44%)
  other arithmetic  113 us (15%)
  blocking collectives  112 us (14%)
  matrix products  97.1 us (12%)
  local copies, waits for them, and re-layouts  86.6 us (11%)
  between operations  13.4 us (2%)
    all_gather x4, blocking collectives, entering(): gathered = jax.tree.map(lambda a: lax.all_gather(a, axis), part)  101 us
    all_gather x1, waiting for transfers between devices, local(): lax.all_gather(switch_projection, 'sp', axis=0, tiled=True)  94.5 us
    all_gather x1, waiting for transfers between devices, local(): lax.all_gather(shrink_projection, 'sp', axis=1, tiled=True)  93.2 us
    all_gather x1, waiting for transfers between devices, local(): lax.all_gather(expand_projection, 'sp', axis=0, tiled=True)  81.1 us
    while x16, local copies, waits for them, and re-layouts  53.2 us
    reduce_scatter x1, waiting for transfers between devices, local(): lax.psum_scatter(jnp.dot(hidden, down_full, preferred_element_type=jnp.fl...  42.9 us
    dot_general x32, other arithmetic, advance(): jnp.einsum('htk,hsk,htsk->hts', block_queries, key_block, decays, precisi...  38.5 us
    exp x32, other arithmetic, advance(): decays = jnp.exp(jnp.where(causal_mask, relative, -jnp.inf))  37.4 us
  transfers between devices with their start and end apart: 5, of which 5 were waited for; matrix products, arithmetic and copies ran while one was open for 2% of the time, Pallas kernels for 0%

commit v1 on v0

v1 whole, which is shorter than its diff:
```python
import functools

import jax
import jax.numpy as jnp
from jax import lax
from jax.experimental import pallas as pl
from jax.experimental.pallas import tpu as pltpu
from jax.sharding import PartitionSpec as P


CHUNK = 128
EPSILON = 1e-06
EXACT = lax.Precision.HIGHEST
F32 = jnp.float32
BF16 = jnp.bfloat16


def nt(a, b):
    return lax.dot_general(a, b, (((1,), (1,)), ((), ())), preferred_element_type=F32)


def tn(a, b):
    return lax.dot_general(a, b, (((0,), (0,)), ((), ())), preferred_element_type=F32)


def front_kernel(
    sp,
    tp,
    q0, f0, gap0, q1, f1, gap1, content, switch, fades, head_scale, source, emission, mlp_scale,
    updated_ref, rows_ref,
    logs0, logs1, fade_cum, state0, state1, run0, run1, intra, out_bound, inbox, mixed, regrouped, full,
    state_send, state_recv, mix_send, mix_recv, far_send, far_recv, near_send, near_recv, put_sem,
):
    sp_me, tp_me = lax.axis_index("sp"), lax.axis_index("tp")
    length = q0.shape[0]
    chunks = length // CHUNK
    block = length // tp
    values = content.shape[2]
    half = values // 2
    groups = ((q0, f0, gap0, logs0, state0, run0), (q1, f1, gap1, logs1, state1, run1))

    barrier = pltpu.get_barrier_semaphore()

    def greet_sp(d, carry):
        pl.semaphore_signal(barrier, inc=1, device_id={"sp": lax.rem(sp_me + d, sp)})
        return carry

    def greet_tp(d, carry):
        pl.semaphore_signal(barrier, inc=1, device_id={"tp": lax.rem(tp_me + d, tp)})
        return carry

    lax.fori_loop(1, sp, greet_sp, 0)
    lax.fori_loop(1, tp, greet_tp, 0)
    pl.semaphore_wait(barrier, sp - 1 + tp - 1)

    row_id = lax.broadcasted_iota(jnp.int32, (CHUNK, CHUNK), 0)
    col_id = lax.broadcasted_iota(jnp.int32, (CHUNK, CHUNK), 1)
    causal = row_id >= col_id
    lower = causal.astype(F32)
    upper = (row_id <= col_id).astype(F32)
    for g in range(2):
        fade_cum[g] = jnp.dot(fades[g], upper, precision=EXACT, preferred_element_type=F32)

    def fade_square(g, c):
        across = jnp.broadcast_to(fade_cum[g, pl.ds(c, 1), :], (CHUNK, CHUNK))
        return across, across.T

    def keys_of(f, gap, rows):
        return gap[...] * jax.nn.sigmoid(-f[rows, :].astype(F32))

    totals = []
    for g, (q, f, gap, logs, state, run) in enumerate(groups):
        width = q.shape[1]
        held = jnp.zeros((values, width), F32)
        passed = jnp.zeros((1, width), F32)
        for c in range(chunks):
            rows = pl.ds(c * CHUNK, CHUNK)
            keys = keys_of(f, gap, rows)
            cum = jnp.dot(lower, jnp.log1p(-keys), precision=EXACT, preferred_element_type=F32)
            logs[rows, :] = cum
            down = fade_square(g, c)[1][:, :width]
            total = cum[CHUNK - 1 :, :] + down[CHUNK - 1 :, :]
            state[c] = held
            run[pl.ds(c, 1), :] = passed
            weighted = (keys * jnp.exp(total - cum - down)).astype(BF16)
            held = jnp.exp(total) * held + tn(content[g, rows, :], weighted)
            passed = passed + total
        totals.append((held, passed))

    (wide, wide_log), (narrow, narrow_log) = totals
    out_bound[0:values, :] = wide.astype(BF16)
    out_bound[values : values + half, :] = jnp.concatenate([narrow[:half], narrow[half:]], axis=1).astype(BF16)
    padded = jnp.concatenate([narrow_log, jnp.zeros_like(narrow_log)], axis=1)
    stack = jnp.concatenate([wide_log, padded], axis=0)
    high = stack.astype(BF16).astype(F32)
    mid = (stack - high).astype(BF16).astype(F32)
    low = stack - high - mid
    out_bound[values + half :, :] = jnp.concatenate(
        [high, mid, low, jnp.zeros((10, values), F32)], axis=0
    ).astype(BF16)

    def state_copy(d, target):
        return pltpu.make_async_remote_copy(
            src_ref=out_bound,
            dst_ref=inbox.at[d - 1],
            send_sem=state_send.at[d - 1],
            recv_sem=state_recv.at[d - 1],
            device_id={"sp": target},
        )

    def send_state(d, carry):
        state_copy(d, sp_me + d).start()
        return carry

    lax.fori_loop(1, sp - sp_me, send_state, 0)

    for g, (q, f, gap, logs, state, run) in enumerate(groups):
        width = q.shape[1]
        for c in range(chunks):
            rows = pl.ds(c * CHUNK, CHUNK)
            cum = logs[rows, :]
            across, down = fade_square(g, c)
            query = jax.nn.silu(q[rows, :].astype(F32)) * (width**-0.5) * jnp.exp(cum)
            keys = keys_of(f, gap, rows) * jnp.exp(-cum)
            scores = nt(query.astype(BF16), keys.astype(BF16))
            decay = jnp.exp(jnp.where(causal, down - across, -jnp.inf))
            inside = jnp.dot((scores * decay).astype(BF16), content[g, rows, :], preferred_element_type=F32)
            intra[g, rows, :] = inside
            logs[rows, :] = query * jnp.exp(down[:, :width])

    def gather_state(d, carry):
        held0, between0, held1, between1 = carry
        state_copy(d, sp_me).wait_recv()
        slot = inbox[d - 1].astype(F32)
        got1 = jnp.concatenate(
            [slot[values : values + half, :half], slot[values : values + half, half:]], axis=0
        )
        base = values + half
        log0 = slot[base : base + 1] + slot[base + 2 : base + 3] + slot[base + 4 : base + 5]
        log1 = slot[base + 1 : base + 2] + slot[base + 3 : base + 4] + slot[base + 5 : base + 6]
        held0 = held0 + jnp.exp(between0) * slot[:values]
        held1 = held1 + jnp.exp(between1) * got1
        return held0, between0 + log0, held1, between1 + log1[:, :half]

    zero = (
        jnp.zeros((values, q0.shape[1]), F32),
        jnp.zeros((1, q0.shape[1]), F32),
        jnp.zeros((values, q1.shape[1]), F32),
        jnp.zeros((1, q1.shape[1]), F32),
    )
    entered0, _, entered1, _ = lax.fori_loop(1, sp_me + 1, gather_state, zero)
    entered = (entered0, entered1)

    def mix_copy(step):
        target = lax.rem(tp_me + step, tp)
        return pltpu.make_async_remote_copy(
            src_ref=mixed.at[target],
            dst_ref=regrouped.at[step - 1],
            send_sem=mix_send.at[step - 1],
            recv_sem=mix_recv.at[step - 1],
            device_id={"tp": target},
        )

    for step in list(range(1, tp)) + [0]:
        owner = lax.rem(tp_me + step, tp)

        def one(i, carry):
            c = owner * (block // CHUNK) + i
            rows = pl.ds(pl.multiple_of(c * CHUNK, CHUNK), CHUNK)
            for g, (q, f, gap, logs, state, run) in enumerate(groups):
                full_state = state[c] + jnp.exp(run[pl.ds(c, 1), :]) * entered[g]
                out = intra[g, rows, :] + nt(logs[rows, :].astype(BF16), full_state.astype(BF16))
                scale = lax.rsqrt(jnp.mean(out * out, axis=1, keepdims=True) + EPSILON)
                gated = out * scale * head_scale[...] * jax.nn.silu(switch[g, rows, :].astype(F32))
                mixed[owner, pl.ds(pl.multiple_of(i * CHUNK, CHUNK), CHUNK), pl.ds(g * values, values)] = gated.astype(BF16)
            return carry

        lax.fori_loop(0, block // CHUNK, one, 0)
        if step:
            mix_copy(step).start()

    width = source.shape[1]
    for step in range(tp):
        owner = lax.rem(tp_me - step + tp, tp)
        if step:
            mix_copy(step).wait_recv()
        for g in range(2):
            part = mixed[owner, :, pl.ds(g * values, values)] if step == 0 else regrouped[step - 1, :, pl.ds(g * values, values)]
            weight = emission[g, pl.ds(pl.multiple_of(owner * values, values), values), :]
            product = jnp.dot(part, weight, preferred_element_type=F32)
            if step == 0 and g == 0:
                updated_ref[...] = source[...].astype(F32) + product
            else:
                updated_ref[...] += product
    new = updated_ref[...]
    inverse = lax.rsqrt(jnp.mean(new * new, axis=1, keepdims=True) + EPSILON)
    full[tp_me] = (new * inverse * mlp_scale[...]).astype(BF16)

    near = tp_me + 1 - 2 * lax.rem(tp_me, 2)
    far_count = tp // 2 - 1

    def far_copy(k):
        return pltpu.make_async_remote_copy(
            src_ref=full.at[tp_me],
            dst_ref=full.at[tp_me],
            send_sem=far_send.at[k - 1],
            recv_sem=far_recv.at[k - 1],
            device_id={"tp": lax.rem(tp_me + 2 * k, tp)},
        )

    def near_copy(k, slot):
        return pltpu.make_async_remote_copy(
            src_ref=full.at[slot],
            dst_ref=full.at[slot],
            send_sem=near_send.at[k],
            recv_sem=near_recv.at[k],
            device_id={"tp": near},
        )

    for k in range(1, far_count + 1):
        far_copy(k).start()
    near_copy(0, tp_me).start()
    for k in range(1, far_count + 1):
        slot = lax.rem(tp_me - 2 * k + tp, tp)
        far_copy(k).wait_recv()
        near_copy(k, slot).start()

    def put(k, slot):
        return pltpu.make_async_copy(full.at[slot], rows_ref.at[slot], put_sem.at[k])

    put(0, tp_me).start()
    for k in range(1, far_count + 1):
        put(k, lax.rem(tp_me - 2 * k + tp, tp)).start()
    for k in range(far_count + 1):
        near_copy(k, tp_me).wait_recv()
        put(far_count + 1 + k, lax.rem(near - 2 * k + tp, tp)).start()
    for k in range(tp):
        put(k, tp_me).wait()

    def drain(d, carry):
        state_copy(d, sp_me).wait_send()
        return carry

    lax.fori_loop(1, sp - sp_me, drain, 0)
    for step in range(1, tp):
        mix_copy(step).wait_send()
    for k in range(1, far_count + 1):
        far_copy(k).wait_send()
    for k in range(far_count + 1):
        near_copy(k, tp_me).wait_send()


def front(sp, tp, source, q0, f0, gap0, q1, f1, gap1, content, switch, fades, head_scale, emission, mlp_scale):
    length = q0.shape[0]
    rows, width = source.shape
    values = content.shape[2]
    block = length // tp
    chunks = length // CHUNK
    packed = values + values // 2 + 16
    far = max(tp // 2 - 1, 1)
    vmem = pl.BlockSpec(memory_space=pltpu.VMEM)
    dma = pltpu.SemaphoreType.DMA
    return pl.pallas_call(
        functools.partial(front_kernel, sp, tp),
        out_shape=(
            jax.ShapeDtypeStruct((rows, width), F32),
            jax.ShapeDtypeStruct((tp, block, width), BF16),
        ),
        in_specs=[vmem] * 13,
        out_specs=(vmem, pl.BlockSpec(memory_space=pl.ANY)),
        scratch_shapes=[
            pltpu.VMEM(q0.shape, F32),
            pltpu.VMEM(q1.shape, F32),
            pltpu.VMEM((2, chunks, CHUNK), F32),
            pltpu.VMEM((chunks, values, q0.shape[1]), F32),
            pltpu.VMEM((chunks, values, q1.shape[1]), F32),
            pltpu.VMEM((chunks, q0.shape[1]), F32),
            pltpu.VMEM((chunks, q1.shape[1]), F32),
            pltpu.VMEM((2, length, values), F32),
            pltpu.VMEM((packed, values), BF16),
            pltpu.VMEM((sp - 1, packed, values), BF16),
            pltpu.VMEM((tp, block, 2 * values), BF16),
            pltpu.VMEM((tp - 1, block, 2 * values), BF16),
            pltpu.VMEM((tp, block, width), BF16),
            dma((sp - 1,)), dma((sp - 1,)),
            dma((tp - 1,)), dma((tp - 1,)),
            dma((far,)), dma((far,)),
            dma((far + 1,)), dma((far + 1,)),
            dma((tp,)),
        ],
        compiler_params=pltpu.CompilerParams(
            collective_id=0, has_side_effects=True, vmem_limit_bytes=48 * 1024 * 1024
        ),
        cost_estimate=pl.CostEstimate(flops=400_000_000_000, bytes_accessed=20_000_000, transcendentals=0),
        name="front",
    )(
        q0, f0, gap0.reshape(1, -1), q1, f1, gap1.reshape(1, -1), content, switch,
        fades.reshape(2, chunks, CHUNK), head_scale.reshape(1, -1), source, emission, mlp_scale.reshape(1, -1),
    )


def local(
    layer_source,
    broad_probe_tensor,
    broad_retention_preact,
    broad_floor_margin,
    slim_probe_tensor,
    slim_retention_preact,
    slim_floor_margin,
    branch_content_tensor,
    emitted_switch_preact,
    extra_log_fades,
    channel_norm_scale,
    emission_projection,
    mlp_norm_scale,
    switch_projection,
    expand_projection,
    shrink_projection,
):
    sp, tp = lax.axis_size("sp"), lax.axis_size("tp")
    gate_full = lax.all_gather(switch_projection, "sp", axis=0, tiled=True)
    up_full = lax.all_gather(expand_projection, "sp", axis=0, tiled=True)
    down_full = lax.all_gather(shrink_projection, "sp", axis=1, tiled=True)
    updated, rows = front(
        sp, tp, layer_source, broad_probe_tensor, broad_retention_preact, broad_floor_margin,
        slim_probe_tensor, slim_retention_preact, slim_floor_margin, branch_content_tensor,
        emitted_switch_preact, extra_log_fades, channel_norm_scale, emission_projection, mlp_norm_scale,
    )
    rows = rows.reshape(-1, rows.shape[2])
    gate_part = jnp.dot(rows, gate_full, preferred_element_type=F32)
    up_part = jnp.dot(rows, up_full, preferred_element_type=F32)
    hidden = (jax.nn.silu(gate_part) * up_part).astype(BF16)
    partial = jnp.dot(hidden, down_full, preferred_element_type=F32).astype(BF16)
    ffn_sum = lax.psum_scatter(partial, "tp", scatter_dimension=0, tiled=True).astype(F32)
    return (updated + 0.5 * ffn_sum).astype(BF16)


def solution(mesh):
    placed = (
        P(("sp", "tp"), None),
        P("sp", "tp"),
        P("sp", "tp"),
        P("tp"),
        P("sp", "tp"),
        P("sp", "tp"),
        P("tp"),
        P(None, "sp", "tp"),
        P(None, "sp", "tp"),
        P(None, "sp", "tp"),
        P(),
        P(),
        P(),
        P("sp", "tp"),
        P("sp", "tp"),
        P("tp", "sp"),
    )
    return jax.shard_map(
        local, mesh=mesh, in_specs=placed, out_specs=P(("sp", "tp"), None), check_vma=False
    )
```

time: 777 us -> 373 us (0.48)
  blocking collectives: 112 us -> 0 us
  other arithmetic: 113 us -> 2.49 us
  waiting for transfers between devices: 345 us -> 262 us
  local copies, waits for them, and re-layouts: 86.6 us -> 10.7 us
  matrix products: 97.1 us -> 32.2 us
  Pallas kernels: 0 us -> 52 us
    all_gather x4 -> x0, blocking collectives: 101 us -> none  [entering(): gathered = jax.tree.map(lambda a: lax.all_gather(a, axis), part)]
    all_gather x4 -> x3, waiting for transfers between devices: 300 us -> 217 us  [the longest x1 92.7 us: local(): up_full = lax.all_gather(expand_projection, 'sp', axis=0, tiled=True)]
    dot_general x101 -> x2, matrix products: 97.1 us -> 32.2 us  [the longest x1 20.6 us: local(): jnp.dot(hidden, down_full, preferred_element_type=F32).astype(BF16)]
    while x16 -> x0, local copies, waits for them, and re-layouts: 53.2 us -> none
    pallas_call x0 -> x1, Pallas kernels: none -> 52 us  [front(): pl.pallas_call(functools.partial(front_kernel, sp, tp), out_shape=(jax.Sh...]
    dot_general x32 -> x0, other arithmetic: 38.5 us -> none  [advance(): jnp.einsum('htk,hsk,htsk->hts', block_queries, key_block, decays, precisi...]
    exp x32 -> x0, other arithmetic: 37.4 us -> none  [advance(): decays = jnp.exp(jnp.where(causal_mask, relative, -jnp.inf))]
    squeeze x64 -> x0, local copies, waits for them, and re-layouts: 24.6 us -> none  [the longest x32 24.5 us: block_recurrence(): lax.scan(advance, initial, (to_blocks(probe_entries), to_blocks(address_e...]
  transfers between devices with their start and end apart: 5 -> 4, of which waited for: 5 -> 4; matrix products, arithmetic and copies ran while one was open for 2% -> 4% of each run, Pallas kernels for 0% -> 14%
where the time goes in v1:
time: 373 us; the launch traced here: 372 us
  waiting for transfers between devices  262 us (70%)
  Pallas kernels  52 us (14%)
  matrix products  32.2 us (9%)
  between operations  13.2 us (4%)
  local copies, waits for them, and re-layouts  10.7 us (3%)
    all_gather x1, waiting for transfers between devices, local(): up_full = lax.all_gather(expand_projection, 'sp', axis=0, tiled=True)  92.7 us
    all_gather x1, waiting for transfers between devices, local(): down_full = lax.all_gather(shrink_projection, 'sp', axis=1, tiled=True)  81.7 us
    pallas_call x1, Pallas kernels, front(): pl.pallas_call(functools.partial(front_kernel, sp, tp), out_shape=(jax.Sh...  52 us
    reduce_scatter x1, waiting for transfers between devices, local(): lax.psum_scatter(partial, 'tp', scatter_dimension=0, tiled=True).astype(F32)  42.9 us
    all_gather x1, waiting for transfers between devices, local(): gate_full = lax.all_gather(switch_projection, 'sp', axis=0, tiled=True)  42.1 us
    dot_general x1, matrix products, local(): jnp.dot(hidden, down_full, preferred_element_type=F32).astype(BF16)  20.6 us
    dot_general x1, matrix products, local(): gate_part = jnp.dot(rows, gate_full, preferred_element_type=F32)  11.6 us
    unnamed x22, local copies, waits for them, and re-layouts  10.7 us
  transfers between devices with their start and end apart: 4, of which 4 were waited for; matrix products, arithmetic and copies ran while one was open for 4% of the time, Pallas kernels for 14%

profile of v1, /device:TPU:0, one launch (start us, length us, event | category | flops | bytes accessed | tf_op | source)
XLA Modules:
  0.0 372.3 jit_solution(16572458945986858384)
XLA Ops:
  6.5 0.0 all-gather.4.cloned.1.call-start
  6.5 0.7 all-gather.4.cloned.1.call-update
  7.3 0.0 all-gather.8.cloned.1.call-start
  7.3 0.7 all-gather.8.cloned.1.call-update
  8.0 0.0 all-gather.6.cloned.1.call-start
  8.1 0.7 all-gather.6.cloned.1.call-update
  8.7 0.0 reduce-scatter.2.cloned.1.call-start
  8.8 1.1 copy.17.q1
  9.9 1.1 copy.18.f1
  10.9 0.0 copy-start
  11.0 1.2 copy-done
  12.2 0.0 copy-start.1
  12.2 1.0 copy-done.1
  13.2 0.0 copy-start.2
  13.2 1.0 copy-done.2
  14.3 0.0 copy-start.3
  14.3 0.9 copy-done.3
  15.2 0.0 copy-start.4
  15.2 0.9 copy-done.4
  16.2 0.0 copy-start.5
  16.2 0.7 copy-done.5
  16.9 0.0 copy-start.6
  16.9 0.7 copy-done.6
  17.6 0.0 copy-start.7
  17.6 0.7 copy-done.7
  18.2 0.0 copy-start.8
  18.2 0.7 copy-done.8
  18.9 0.0 copy-start.9
  18.9 0.7 copy-done.9
  19.5 52.0 %front.1 = (f32[256,2048]{1,0:T(8,128)S(1)}, bf16[4,256,2048]{2,1,0:T(8,128)(2,1)}) custom-call(bf16[1024,128]{1,0:T(8,128)(2,1)S(1)} %copy-done.3, bf16[1024,128]{1,0:T(8,128)(2,1)S(1)} %copy-done.4, f32[1,128]{1,0:T(1,128)S(1)} %bitcast.22, bf16[1024,64]{1,0:T(8,128)(2,1)S(1)} %copy.17.q1, bf16[1024,64]{1,0:T(8,128)(2,1)S(1)} %copy.18.f1, ...), custom_call_target="tpu_custom_call" | custom-call | flops 399999991808 | bytes 20000000 | tf_op jit(solution)/shard_map/front/pallas_call | solution.py:263
  71.6 42.1 %all-gather.4.cloned.1.call-done = bf16[2048,1408]{1,0:T(8,128)(2,1)} async-done(((bf16[256,1408]{1,0:T(8,128)(2,1)}), bf16[2048,1408]{1,0:T(8,128)(2,1)}) %all-gather.4.cloned.1.call-update) | async-done | bytes 5767184 | tf_op jit(solution)/shard_map/all_gather | solution.py:321
  113.6 11.6 %fusion = f32[1024,1408]{1,0:T(8,128)} fusion(bf16[1024,2048]{1,0:T(8,128)(2,1)} %bitcast.25, bf16[2048,1408]{1,0:T(8,128)(2,1)} %all-gather.4.cloned.1.call-done), kind=kOutput, calls=%fused_computation.3 | convolution fusion | flops 5905580032 | bytes 15728640 | tf_op jit(solution)/shard_map/dot_general | solution.py:330
  125.3 81.7 %all-gather.8.cloned.1.call-done = bf16[1408,2048]{1,0:T(8,128)(2,1)} async-done(((bf16[1408,256]{1,0:T(8,128)(2,1)}), bf16[1408,2048]{1,0:T(8,128)(2,1)}) %all-gather.8.cloned.1.call-update) | async-done | bytes 5767184 | tf_op jit(solution)/shard_map/all_gather | solution.py:323
  207.0 92.7 %all-gather.6.cloned.1.call-done = bf16[2048,1408]{1,0:T(8,128)(2,1)} async-done(((bf16[256,1408]{1,0:T(8,128)(2,1)}), bf16[2048,1408]{1,0:T(8,128)(2,1)}) %all-gather.6.cloned.1.call-update) | async-done | bytes 5767184 | tf_op jit(solution)/shard_map/all_gather | solution.py:322
  299.7 20.6 %convolution_convert_fusion = bf16[1024,2048]{1,0:T(8,128)(2,1)} fusion(bf16[1408,2048]{1,0:T(8,128)(2,1)} %all-gather.8.cloned.1.call-done, f32[1024,1408]{1,0:T(8,128)} %fusion, bf16[1024,2048]{1,0:T(8,128)(2,1)} %bitcast.26, bf16[2048,1408]{1,0:T(8,128)(2,1)} %all-gather.6.cloned.1.call-done), kind=kOutput, calls=%fused_computation.1 | convolution fusion | flops 11821907968 | bytes 25690112 | tf_op jit(solution)/shard_map/dot_general | solution.py:333
  320.3 0.0 reduce-scatter.2.cloned.1.call-update
  320.3 42.9 %reduce-scatter.2.cloned.1.call-done = bf16[256,2048]{1,0:T(8,128)(2,1)} async-done(((bf16[1024,2048]{1,0:T(8,128)(2,1)}), bf16[256,2048]{1,0:T(8,128)(2,1)}) %reduce-scatter.2.cloned.1.call-update) | async-done | bytes 1048592 | tf_op jit(solution)/shard_map/reduce_scatter | solution.py:334
  363.3 2.5 add_convert_fusion
Async XLA Ops:
  6.5 107.1 %all-gather.4.cloned.1.call-start = ((), (), s32[]{:S(2)}) async-start(), calls=%async_computation.1 | async-start | bytes 6488064 | tf_op jit(solution)/shard_map/all_gather | solution.py:321
  7.3 199.8 %all-gather.8.cloned.1.call-start = ((), (), s32[]{:S(2)}) async-start(), calls=%async_computation.3 | async-start | bytes 6488064 | tf_op jit(solution)/shard_map/all_gather | solution.py:323
  8.0 291.7 %all-gather.6.cloned.1.call-start = ((), (), s32[]{:S(2)}) async-start(), calls=%async_computation.2 | async-start | bytes 6488064 | tf_op jit(solution)/shard_map/all_gather | solution.py:322
  8.7 354.5 %reduce-scatter.2.cloned.1.call-start = ((), (), s32[]{:S(2)}) async-start(), calls=%async_computation.4 | async-start | bytes 5242880 | tf_op jit(solution)/shard_map/reduce_scatter | solution.py:334
  10.9 1.2 copy-start
  12.2 1.0 copy-start.1
  13.2 1.0 copy-start.2
  14.3 0.9 copy-start.3
  15.2 0.9 copy-start.4
  16.2 0.7 copy-start.5
  16.9 0.7 copy-start.6
  17.6 0.7 copy-start.7
  18.2 0.7 copy-start.8
  18.9 0.7 copy-start.9
Sparse Core Ops, SparseCore 0:
  9.5 104.0 all-gather.3
  115.7 91.2 all-gather.7
  209.2 90.4 all-gather.5
  320.5 42.7 reduce-scatter.1

commit v2 on v1

--- a/solution.py
+++ b/solution.py
@@ -318,18 +318,33 @@
     shrink_projection,
 ):
     sp, tp = lax.axis_size("sp"), lax.axis_size("tp")
-    gate_full = lax.all_gather(switch_projection, "sp", axis=0, tiled=True)
-    up_full = lax.all_gather(expand_projection, "sp", axis=0, tiled=True)
+    groups = [[i for i in range(sp) if i % 2 == r] for r in range(2)]
+    swap = [(i, i ^ 1) for i in range(sp)]
+    gate_own = lax.all_gather(switch_projection, "sp", axis=0, tiled=True, axis_index_groups=groups)
+    up_own = lax.all_gather(expand_projection, "sp", axis=0, tiled=True, axis_index_groups=groups)
     down_full = lax.all_gather(shrink_projection, "sp", axis=1, tiled=True)
     updated, rows = front(
         sp, tp, layer_source, broad_probe_tensor, broad_retention_preact, broad_floor_margin,
         slim_probe_tensor, slim_retention_preact, slim_floor_margin, branch_content_tensor,
         emitted_switch_preact, extra_log_fades, channel_norm_scale, emission_projection, mlp_norm_scale,
     )
-    rows = rows.reshape(-1, rows.shape[2])
-    gate_part = jnp.dot(rows, gate_full, preferred_element_type=F32)
-    up_part = jnp.dot(rows, up_full, preferred_element_type=F32)
+    gate_other = lax.ppermute(gate_own, "sp", swap)
+    up_other = lax.ppermute(up_own, "sp", swap)
+    piece = switch_projection.shape[0]
+    parity = lax.rem(lax.axis_index("sp"), 2)
+    pieces = rows.reshape(-1, sp // 2, 2, piece)
+
+    def columns(which):
+        picked = lax.dynamic_index_in_dim(pieces, which, 2, False)
+        return picked.reshape(picked.shape[0], -1)
+
+    own, other = lax.optimization_barrier((columns(parity), columns(1 - parity)))
+    gate_part = jnp.dot(own, gate_own, preferred_element_type=F32)
+    gate_part = gate_part + jnp.dot(other, gate_other, preferred_element_type=F32)
+    up_part = jnp.dot(own, up_own, preferred_element_type=F32)
+    up_part = up_part + jnp.dot(other, up_other, preferred_element_type=F32)
     hidden = (jax.nn.silu(gate_part) * up_part).astype(BF16)
+    hidden = lax.optimization_barrier(hidden)
     partial = jnp.dot(hidden, down_full, preferred_element_type=F32).astype(BF16)
     ffn_sum = lax.psum_scatter(partial, "tp", scatter_dimension=0, tiled=True).astype(F32)
     return (updated + 0.5 * ffn_sum).astype(BF16)

time: 373 us -> 399 us (1.070)
  waiting for transfers between devices: 262 us -> 204 us
  Pallas kernels: 52 us -> 92.7 us
  local copies, waits for them, and re-layouts: 10.7 us -> 45.8 us
  matrix products: 32.2 us -> 36.6 us
    all_gather x1, waiting for transfers between devices: 81.7 us -> 0.01 us  [local(): down_full = lax.all_gather(shrink_projection, 'sp', axis=1, tiled=True)]
    reduce_scatter x1, waiting for transfers between devices: 42.9 us -> 84.1 us  [local(): lax.psum_scatter(partial, 'tp', scatter_dimension=0, tiled=True).astype(F32)]
    pallas_call x1, Pallas kernels: 52 us -> 92.7 us  [front(): pl.pallas_call(functools.partial(front_kernel, sp, tp), out_shape=(jax.Sh...]
    all_gather x2, waiting for transfers between devices: 135 us -> 118 us  [the longest x1 59.8 us: local(): lax.all_gather(switch_projection, 'sp', axis=0, tiled=True, axis_index_gr...]
    unnamed x22 -> x30, local copies, waits for them, and re-layouts: 10.7 us -> 26.5 us
    dot_general x1 -> x4, matrix products: 11.6 us -> 25.7 us  [the longest x1 8.89 us: local(): up_part = up_part + jnp.dot(other, up_other, preferred_element_type=F32)]
    dynamic_slice x0 -> x1, local copies, waits for them, and re-layouts: none -> 11.5 us  [columns(): picked = lax.dynamic_index_in_dim(pieces, which, 2, False)]
    dot_general x1, matrix products: 20.6 us -> 10.9 us  [local(): jnp.dot(hidden, down_full, preferred_element_type=F32).astype(BF16)]
  transfers between devices with their start and end apart: 4 -> 6, of which waited for: 4 -> 3; matrix products, arithmetic and copies ran while one was open for 4% -> 17% of each run, Pallas kernels for 14% -> 23%
where the time goes in v2:
time: 399 us; the launch traced here: 398 us
  waiting for transfers between devices  204 us (51%)
  Pallas kernels  92.7 us (23%)
  local copies, waits for them, and re-layouts  45.8 us (11%)
  matrix products  36.6 us (9%)
  between operations  13.3 us (3%)
    pallas_call x1, Pallas kernels, front(): pl.pallas_call(functools.partial(front_kernel, sp, tp), out_shape=(jax.Sh...  92.7 us
    reduce_scatter x1, waiting for transfers between devices, local(): lax.psum_scatter(partial, 'tp', scatter_dimension=0, tiled=True).astype(F32)  84.1 us
    all_gather x1, waiting for transfers between devices, local(): lax.all_gather(switch_projection, 'sp', axis=0, tiled=True, axis_index_gr...  59.8 us
    all_gather x1, waiting for transfers between devices, local(): lax.all_gather(expand_projection, 'sp', axis=0, tiled=True, axis_index_gr...  57.9 us
    unnamed x30, local copies, waits for them, and re-layouts  26.5 us
    dynamic_slice x1, local copies, waits for them, and re-layouts, columns(): picked = lax.dynamic_index_in_dim(pieces, which, 2, False)  11.5 us
    dot_general x1, matrix products, local(): jnp.dot(hidden, down_full, preferred_element_type=F32).astype(BF16)  10.9 us
    dot_general x1, matrix products, local(): up_part = up_part + jnp.dot(other, up_other, preferred_element_type=F32)  8.89 us
  transfers between devices with their start and end apart: 6, of which 3 were waited for; matrix products, arithmetic and copies ran while one was open for 17% of the time, Pallas kernels for 23%

profile of v2, /device:TPU:0, one launch (start us, length us, event | category | flops | bytes accessed | tf_op | source)
XLA Modules:
  0.0 397.9 jit_solution(11784171830408245601)
XLA Ops:
  6.5 0.0 copy-start.3
  6.5 0.0 copy-start.7
  6.5 0.0 copy-start.8
  6.5 0.0 copy-start.1
  6.5 0.0 copy-start.5
  6.5 0.0 copy-start.9
  6.6 0.0 copy-start.6
  6.6 0.0 all-gather.4.cloned.1.call-start
  6.6 0.7 all-gather.4.cloned.1.call-update
  7.3 0.0 all-gather.6.cloned.1.call-start
  7.3 0.7 all-gather.6.cloned.1.call-update
  8.1 0.0 all-gather.8.cloned.1.call-start
  8.1 0.7 all-gather.8.cloned.1.call-update
  8.8 0.0 reduce-scatter.2.cloned.1.call-start
  8.8 1.1 copy.19.q1
  9.9 1.1 copy.20.f1
  11.0 59.8 %all-gather.4.cloned.1.call-done = bf16[1024,1408]{1,0:T(8,128)(2,1)} async-done(((bf16[256,1408]{1,0:T(8,128)(2,1)}), bf16[1024,1408]{1,0:T(8,128)(2,1)}) %all-gather.4.cloned.1.call-update) | async-done | bytes 2883600 | tf_op jit(solution)/shard_map/all_gather | solution.py:323
  70.8 1.5 collective-permute-start
  72.3 57.9 %all-gather.6.cloned.1.call-done = bf16[1024,1408]{1,0:T(8,128)(2,1)} async-done(((bf16[256,1408]{1,0:T(8,128)(2,1)}), bf16[1024,1408]{1,0:T(8,128)(2,1)}) %all-gather.6.cloned.1.call-update) | async-done | bytes 2883600 | tf_op jit(solution)/shard_map/all_gather | solution.py:324
  130.2 1.5 collective-permute-start.1
  131.7 0.0 copy-done.3
  131.7 0.0 copy-done.7
  131.7 0.0 copy-done.8
  131.7 0.0 copy-done.1
  131.7 0.0 copy-done.5
  131.7 0.0 copy-done.9
  131.7 0.0 copy-done.6
  131.7 0.0 copy-start
  131.7 1.2 copy-done
  133.0 0.0 copy-start.2
  133.0 1.0 copy-done.2
  134.0 0.0 copy-start.4
  134.0 0.9 copy-done.4
  135.0 92.7 %front.1 = (f32[256,2048]{1,0:T(8,128)S(1)}, bf16[4,256,2048]{2,1,0:T(8,128)(2,1)}) custom-call(bf16[1024,128]{1,0:T(8,128)(2,1)S(1)} %copy-done.3, bf16[1024,128]{1,0:T(8,128)(2,1)S(1)} %copy-done.4, f32[1,128]{1,0:T(1,128)S(1)} %bitcast.19, bf16[1024,64]{1,0:T(8,128)(2,1)S(1)} %copy.19.q1, bf16[1024,64]{1,0:T(8,128)(2,1)S(1)} %copy.20.f1, ...), custom_call_target="tpu_custom_call" | custom-call | flops 399999991808 | bytes 20000000 | tf_op jit(solution)/shard_map/front/pallas_call | solution.py:263
  227.6 7.8 %reshape.31 = bf16[1024,4,2,256]{3,2,1,0:T(2,128)(2,1)} reshape(bf16[4,256,2048]{2,1,0:T(8,128)(2,1)} %get-tuple-element.10) | data formatting | bytes 8388608 | tf_op jit(solution)/shard_map/reshape | solution.py:335
  235.5 11.5 %constant_dynamic-slice_fusion = (bf16[1024,4,1,256]{3,2,1,0:T(2,128)(2,1)}, bf16[1024,4,1,256]{3,2,1,0:T(2,128)(2,1)}) fusion(bf16[1024,4,2,256]{3,2,1,0:T(2,128)(2,1)} %reshape.31, s32[]{:T(128)S(6)} %select_n.8, s32[]{:T(128)S(6)} %select_n.7), kind=kLoop, calls=%fused_computation.3 | loop fusion | bytes 8388616 | tf_op jit(solution)/shard_map/jit(dynamic_index_in_dim)/dynamic_slice | solution.py:338
  246.9 10.6 %copy.23 = bf16[1024,4,1,256]{0,3,1,2:T(8,128)(2,1)} copy(bf16[1024,4,1,256]{3,2,1,0:T(2,128)(2,1)} %get-tuple-element.14) | data formatting | bytes 4194304
  257.5 10.6 %copy.24 = bf16[1024,4,1,256]{0,3,1,2:T(8,128)(2,1)} copy(bf16[1024,4,1,256]{3,2,1,0:T(2,128)(2,1)} %get-tuple-element.13) | data formatting | bytes 4194304
  268.1 0.0 copy-start.11
  268.1 0.0 copy-start.12
  268.1 6.1 %fusion.2 = f32[1024,1408]{1,0:T(8,128)S(1)} fusion(bf16[1024,1024]{0,1:T(8,128)(2,1)} %bitcast.24, bf16[1024,1408]{1,0:T(8,128)(2,1)} %all-gather.6.cloned.1.call-done), kind=kOutput, calls=%fused_computation.7 | convolution fusion | flops 2952790016 | bytes 10747904 | tf_op jit(solution)/shard_map/dot_general | solution.py:344
  274.2 0.0 copy-done.11
  274.2 0.0 copy-done.12
  274.2 0.0 copy-start.10
  274.2 3.5 fusion
  277.7 0.0 collective-permute-done
  277.8 0.0 copy-done.10
  277.8 7.1 %fusion.1 = f32[1024,1408]{1,0:T(8,128)} fusion(bf16[1024,1024]{0,1:T(8,128)(2,1)S(1)} %bitcast.22, bf16[1024,1408]{1,0:T(8,128)(2,1)} %collective-permute-done), kind=kOutput, calls=%fused_computation.6 | convolution fusion | flops 2952790016 | bytes 10747904 | tf_op jit(solution)/shard_map/dot_general | solution.py:343
  284.9 0.0 collective-permute-done.1
  284.9 8.9 %multiply_convert_fusion = bf16[1024,1408]{1,0:T(8,128)(2,1)} fusion(f32[1024,1408]{1,0:T(8,128)S(1)} %fusion.2, f32[1024,1408]{1,0:T(8,128)S(1)} %fusion, f32[1024,1408]{1,0:T(8,128)} %fusion.1, bf16[1024,1024]{0,1:T(8,128)(2,1)S(1)} %bitcast.23, bf16[1024,1408]{1,0:T(8,128)(2,1)} %collective-permute-done.1), kind=kOutput, calls=%fused_computation | convolution fusion | flops 2964324352 | bytes 25165824 | tf_op jit(solution)/shard_map/dot_general | solution.py:345
  293.8 0.0 all-gather.8.cloned.1.call-done
  293.8 10.9 %convolution_convert_fusion = bf16[1024,2048]{1,0:T(8,128)(2,1)} fusion(bf16[1024,1408]{1,0:T(8,128)(2,1)} %multiply_convert_fusion, bf16[1408,2048]{1,0:T(8,128)(2,1)} %all-gather.8.cloned.1.call-done), kind=kOutput, calls=%fused_computation.1 | convolution fusion | flops 5907677184 | bytes 12845056 | tf_op jit(solution)/shard_map/dot_general | solution.py:348
  304.7 0.0 reduce-scatter.2.cloned.1.call-update
  304.8 84.1 %reduce-scatter.2.cloned.1.call-done = bf16[256,2048]{1,0:T(8,128)(2,1)} async-done(((bf16[1024,2048]{1,0:T(8,128)(2,1)}), bf16[256,2048]{1,0:T(8,128)(2,1)}) %reduce-scatter.2.cloned.1.call-update) | async-done | bytes 1048592 | tf_op jit(solution)/shard_map/reduce_scatter | solution.py:349
  388.9 2.5 add_convert_fusion
Async XLA Ops:
  6.5 125.2 %copy-start.3 = (bf16[1024,128]{1,0:T(8,128)(2,1)S(1)}, bf16[1024,128]{1,0:T(8,128)(2,1)}, u32[]{:S(2)}) copy-start(bf16[1024,128]{1,0:T(8,128)(2,1)} %q0.1) | copy-start | bytes 786436
  6.5 125.2 %copy-start.7 = (f32[128]{0:T(128)S(1)}, f32[128]{0:T(128)}, u32[]{:S(2)}) copy-start(f32[128]{0:T(128)} %param.19) | copy-start | bytes 1540
  6.5 125.2 %copy-start.8 = (f32[64]{0:T(128)S(1)}, f32[64]{0:T(128)}, u32[]{:S(2)}) copy-start(f32[64]{0:T(128)} %param.22) | copy-start | bytes 772
  6.5 125.2 %copy-start.1 = (bf16[2,1024,128]{2,1,0:T(8,128)(2,1)S(1)}, bf16[2,1024,128]{2,1,0:T(8,128)(2,1)}, u32[]{:S(2)}) copy-start(bf16[2,1024,128]{2,1,0:T(8,128)(2,1)} %content.1) | copy-start | bytes 1572868
  6.5 125.2 %copy-start.5 = (f32[2,1024,1]{1,2,0:T(1,128)S(1)}, f32[2,1024,1]{1,2,0:T(1,128)}, u32[]{:S(2)}) copy-start(f32[2,1024,1]{1,2,0:T(1,128)} %param.25) | copy-start | bytes 24580
  6.5 125.2 %copy-start.9 = (f32[128]{0:T(128)S(1)}, f32[128]{0:T(128)}, u32[]{:S(2)}) copy-start(f32[128]{0:T(128)} %param.26) | copy-start | bytes 1540
  6.6 125.2 %copy-start.6 = (f32[2048]{0:T(1024)S(1)}, f32[2048]{0:T(1024)}, u32[]{:S(2)}) copy-start(f32[2048]{0:T(1024)} %param.28) | copy-start | bytes 24580
  6.6 64.2 %all-gather.4.cloned.1.call-start = ((), (), s32[]{:S(2)}) async-start(), calls=%async_computation.1 | async-start | bytes 3604480 | tf_op jit(solution)/shard_map/all_gather | solution.py:323
  7.3 122.9 %all-gather.6.cloned.1.call-start = ((), (), s32[]{:S(2)}) async-start(), calls=%async_computation.2 | async-start | bytes 3604480 | tf_op jit(solution)/shard_map/all_gather | solution.py:324
  8.1 285.7 %all-gather.8.cloned.1.call-start = ((), (), s32[]{:S(2)}) async-start(), calls=%async_computation.3 | async-start | bytes 6488064 | tf_op jit(solution)/shard_map/all_gather | solution.py:325
  8.8 380.1 %reduce-scatter.2.cloned.1.call-start = ((), (), s32[]{:S(2)}) async-start(), calls=%async_computation.4 | async-start | bytes 5242880 | tf_op jit(solution)/shard_map/reduce_scatter | solution.py:349
  70.8 206.9 %collective-permute-start = (bf16[1024,1408]{1,0:T(8,128)(2,1)}, bf16[1024,1408]{1,0:T(8,128)(2,1)}, u32[]{:S(2)}, u32[]{:S(2)}) collective-permute-start(bf16[1024,1408]{1,0:T(8,128)(2,1)} %all-gather.4.cloned.1.call-done), channel_id=1, source_target_pairs={{0,4},{4,0},{8,12},{12,8},{16,20},{20,16},{24,28},{28,24},{1,5},{5... | collective-permute-start | bytes 8650760 | tf_op jit(solution)/shard_map/ppermute | solution.py:331
  130.2 154.7 %collective-permute-start.1 = (bf16[1024,1408]{1,0:T(8,128)(2,1)}, bf16[1024,1408]{1,0:T(8,128)(2,1)}, u32[]{:S(2)}, u32[]{:S(2)}) collective-permute-start(bf16[1024,1408]{1,0:T(8,128)(2,1)} %all-gather.6.cloned.1.call-done), channel_id=1, source_target_pairs={{0,4},{4,0},{8,12},{12,8},{16,20},{20,16},{24,28},{28,24},{1,5},{5... | collective-permute-start | bytes 8650760 | tf_op jit(solution)/shard_map/ppermute | solution.py:332
  131.7 1.2 copy-start
  133.0 1.0 copy-start.2
  134.0 0.9 copy-start.4
  268.1 6.1 %copy-start.11 = (bf16[1024,4,1,256]{0,3,1,2:T(8,128)(2,1)S(1)}, bf16[1024,4,1,256]{0,3,1,2:T(8,128)(2,1)}, u32[]{:S(2)}) copy-start(bf16[1024,4,1,256]{0,3,1,2:T(8,128)(2,1)} %copy.23) | copy-start | bytes 6291460
  268.1 6.1 %copy-start.12 = (bf16[1024,1408]{1,0:T(8,128)(2,1)S(1)}, bf16[1024,1408]{1,0:T(8,128)(2,1)}, u32[]{:S(2)}) copy-start(bf16[1024,1408]{1,0:T(8,128)(2,1)} %all-gather.4.cloned.1.call-done) | copy-start | bytes 8650756
  274.2 3.5 copy-start.10
Sparse Core Ops, SparseCore 0:
  8.9 61.8 all-gather.3
  72.4 57.7 all-gather.5
  132.3 123.6 all-gather.7
  304.9 83.9 reduce-scatter.1
